TPU v7x, 32 devices: a whole 2x2x4 slice. The times are simulated.
32 devices in a mesh: dp: 4 (over y, x), kv: 4 (over z), tp: 2 (over core).
Axes of the slice: x: 2, y: 2, z: 4, core: 2. Of those that a mesh axis runs over, the one named last changes fastest.
Arguments:
- hidden: bfloat16 [2048, 16], P(('kv', 'tp'), 'dp'), parts along dimension 1, may hold values from -20 to 20
- mixer_gain: float32 [2048], replicated, may hold values from 0.1 to 1.9
- gate_proj: bfloat16 [2048, 64, 64], P(None, 'kv', 'tp'), may hold values from -0.125 to 0.125
- inner_proj: bfloat16 [2048, 64, 64], P(None, 'kv', 'tp'), may hold values from -0.125 to 0.125
- input_proj: bfloat16 [2048, 1024], P(None, 'kv'), may hold values from -0.125 to 0.125
- output_proj: bfloat16 [2048, 1024], P(None, 'kv'), may hold values from -0.125 to 0.125
- step_proj: bfloat16 [2048, 64], replicated, may hold values from -0.125 to 0.125
- step_bias: float32 [64], replicated, may hold values from -3 to -0.5
- decay_log: float32 [64], replicated, may hold values from -3 to 1
- skip_gain: float32 [64], replicated, may hold values from 0.3 to 1.5
- taps_inner: float32 [4, 64, 64], P(None, None, 'tp'), may hold values from -3 to 3
- taps_input: float32 [4, 1024], replicated, may hold values from -3 to 3
- taps_output: float32 [4, 1024], replicated, may hold values from -3 to 3
- recent_inner: bfloat16 [16, 3, 64, 64], P(('dp', 'kv'), None, None, 'tp'), parts along dimension 0, may hold values from -6 to 6
- recent_input: bfloat16 [16, 3, 1024], P(('dp', 'kv')), parts along dimension 0, may hold values from -6 to 6
- recent_output: bfloat16 [16, 3, 1024], P(('dp', 'kv')), parts along dimension 0, may hold values from -6 to 6
- states: float32 [16, 64, 64, 128], P(('dp', 'kv'), None, 'tp'), parts along dimension 0, may hold values from -4 to 4
- block_inner: bfloat16 [16, 128, 64, 64], P(('dp', 'kv'), None, None, 'tp'), parts along dimension 0, may hold values from -6 to 6
- block_input: bfloat16 [16, 128, 1024], P(('dp', 'kv')), parts along dimension 0, may hold values from -4 to 4
- block_decay: float32 [16, 128, 64], P(('dp', 'kv')), parts along dimension 0
- lengths: int32 [16], P(('dp', 'kv')), parts along dimension 0, may hold values from 1 to 128, 170 in all
- norm_gain: float32 [64, 64], P(None, 'tp'), may hold values from 0.1 to 1.9
- mixer_out: bfloat16 [64, 64, 2048], P('kv', 'tp'), may hold values from -0.125 to 0.125
- channel_gain: float32 [2048], replicated, may hold values from 0.1 to 1.9
- expand_gate: bfloat16 [2048, 5632], P(None, ('kv', 'tp')), may hold values from -0.125 to 0.125
- expand_value: bfloat16 [2048, 5632], P(None, ('kv', 'tp')), may hold values from -0.125 to 0.125
- reduce_proj: bfloat16 [5632, 2048], P(('kv', 'tp')), may hold values from -0.109375 to 0.109375
Outputs:
- layer_out: bfloat16 [2048, 16], P(('kv', 'tp'), 'dp'), parts along dimension 1
There are 4 independent parts, one for each index of `dp`. A program takes and returns all parts, laid end to end along the dimension named above; an argument that names none is the same for every part. Nothing has to cross between parts.
All inputs are finite; a program needn't handle non-finite values. No bound on the sum of `lengths` on one device may be relied on, other than what follows from the above.
Results may differ from a plain program's by a relative error of at most 0.01.
Values may be sent and summed in bfloat16 or wider, within the bound.
A program may use at most 64 MiB of HBM per device.

v0:
```python
import jax
import jax.numpy as jnp
from jax import lax
from jax.sharding import PartitionSpec as P

MIXER_HEADS = 64
HEAD_DIM = 64
GROUPS = 8
STATE = 128
OPEN_BLOCK_SPAN = 128


epsilon = 1e-05


def short_conv(recent, newest, taps):
    window = jnp.concatenate(
        [recent.astype(jnp.float32), newest.astype(jnp.float32)[:, None]], axis=1
    )
    return jax.nn.silu(jnp.sum(window * taps[None], axis=1))


def shards(
    hidden,
    mixer_gain,
    gate_proj,
    inner_proj,
    input_proj,
    output_proj,
    step_proj,
    step_bias,
    decay_log,
    skip_gain,
    taps_inner,
    taps_input,
    taps_output,
    recent_inner,
    recent_input,
    recent_output,
    states,
    block_inner,
    block_input,
    block_decay,
    lengths,
    norm_gain,
    mixer_out,
    channel_gain,
    expand_gate,
    expand_value,
    reduce_proj,
):
    rows_own = hidden.shape[0]
    seq_all = hidden.shape[1]
    seq_dev = states.shape[0]
    half_dim = states.shape[2]
    width = rows_own * lax.axis_size("kv") * lax.axis_size("tp")
    offset = (lax.axis_index("kv") * lax.axis_size("tp") + lax.axis_index("tp")) * rows_own
    own_start = lax.axis_index("kv") * seq_dev
    whole_rows = lax.all_gather(hidden, ("kv", "tp"), axis=0, tiled=True)
    whole_f = whole_rows.astype(jnp.float32)
    rms_in = lax.rsqrt(jnp.mean(whole_f * whole_f, axis=0) + epsilon)
    normed_in = (whole_f * mixer_gain[:, None]).astype(jnp.bfloat16)
    gate_part = (
        rms_in[:, None, None]
        * jnp.einsum("ds,dhp->shp", normed_in, gate_proj, preferred_element_type=jnp.float32)
    ).astype(jnp.bfloat16)
    inner_part = (
        rms_in[:, None, None]
        * jnp.einsum("ds,dhp->shp", normed_in, inner_proj, preferred_element_type=jnp.float32)
    ).astype(jnp.bfloat16)
    input_part = (
        rms_in[:, None]
        * jnp.einsum("ds,dk->sk", normed_in, input_proj, preferred_element_type=jnp.float32)
    ).astype(jnp.bfloat16)
    output_part = (
        rms_in[:, None]
        * jnp.einsum("ds,dk->sk", normed_in, output_proj, preferred_element_type=jnp.float32)
    ).astype(jnp.bfloat16)
    own_cols = lax.dynamic_slice_in_dim(normed_in, own_start, seq_dev, 1)
    own_rms = lax.dynamic_slice_in_dim(rms_in, own_start, seq_dev, 0)
    step_pre = (
        own_rms[:, None]
        * jnp.einsum("ds,dh->sh", own_cols, step_proj, preferred_element_type=jnp.float32)
    ).astype(jnp.bfloat16)
    gate_pre, inner_pre, input_pre, output_pre = (
        lax.all_to_all(gate_part, "kv", split_axis=0, concat_axis=1, tiled=True),
        lax.all_to_all(inner_part, "kv", split_axis=0, concat_axis=1, tiled=True),
        lax.all_to_all(input_part, "kv", split_axis=0, concat_axis=1, tiled=True),
        lax.all_to_all(output_part, "kv", split_axis=0, concat_axis=1, tiled=True),
    )
    conv_inner = short_conv(recent_inner, inner_pre, taps_inner)
    conv_input = short_conv(recent_input, input_pre, taps_input)
    conv_output = short_conv(recent_output, output_pre, taps_output).astype(jnp.bfloat16)
    step = jax.nn.softplus(step_pre.astype(jnp.float32) + step_bias[None, :])
    new_decay = -jnp.exp(decay_log)[None, :] * step
    per_group = MIXER_HEADS // GROUPS
    live = (jnp.arange(OPEN_BLOCK_SPAN, dtype=jnp.int32)[None, :] < lengths[:, None]).astype(
        jnp.float32
    )
    masked = block_decay * live[:, :, None]
    cached = jnp.sum(masked, axis=1)
    tail = new_decay[:, None, :] + cached[:, None, :] - jnp.cumsum(masked, axis=1)
    total = new_decay + cached
    readout = conv_output.reshape(seq_dev, GROUPS, STATE)
    score = jnp.einsum(
        "sgn,sjgn->sgj",
        readout,
        block_input.reshape(seq_dev, OPEN_BLOCK_SPAN, GROUPS, STATE),
        preferred_element_type=jnp.float32,
    )
    score_heads = jnp.repeat(score, per_group, axis=1)
    weight = (live[:, None, :] * jnp.exp(jnp.swapaxes(tail, 1, 2)) * score_heads).astype(
        jnp.bfloat16
    )
    from_block = jnp.einsum(
        "shj,sjhp->shp", weight, block_inner, preferred_element_type=jnp.float32
    )
    readout_f = readout.astype(jnp.float32)
    grouped = states.reshape(seq_dev, GROUPS, per_group, half_dim, STATE)
    from_state = jnp.einsum(
        "sgn,sgrpn->sgrp", readout_f, grouped, precision=lax.Precision.HIGHEST
    ).reshape(seq_dev, MIXER_HEADS, half_dim)
    own_score = jnp.repeat(
        jnp.sum(readout_f * conv_input.reshape(seq_dev, GROUPS, STATE), axis=-1), per_group, axis=1
    )
    mix = (
        from_block
        + jnp.exp(total)[:, :, None] * from_state
        + (own_score * step)[:, :, None] * conv_inner
        + skip_gain[None, :, None] * conv_inner
    )
    gated_raw = mix * jax.nn.silu(gate_pre.astype(jnp.float32))
    part_squares = jnp.sum(gated_raw * gated_raw, axis=(1, 2))
    gated = (gated_raw * norm_gain[None]).astype(jnp.bfloat16)
    placed = lax.dynamic_update_slice_in_dim(
        jnp.zeros((seq_all,), jnp.float32), part_squares, own_start, 0
    )
    gate_squares = lax.psum(placed, ("kv", "tp"))
    rms_gate = lax.rsqrt(gate_squares / (MIXER_HEADS * HEAD_DIM) + epsilon)
    by_head = lax.all_to_all(gated, "kv", split_axis=1, concat_axis=0, tiled=True)
    columns = mixer_out
    mixed_full = rms_gate[None, :] * lax.psum(
        jnp.einsum("hpd,shp->ds", columns, by_head, preferred_element_type=jnp.float32),
        ("kv", "tp"),
    )
    mid_full = (whole_f + mixed_full).astype(jnp.bfloat16)
    mid = lax.dynamic_slice_in_dim(mid_full, offset, rows_own, 0)
    full_f = mid_full.astype(jnp.float32)
    mid_squares = jnp.sum(full_f * full_f, axis=0)
    normed_full = (full_f * channel_gain[:, None]).astype(jnp.bfloat16)
    gate_sum = jnp.einsum("ds,df->sf", normed_full, expand_gate, preferred_element_type=jnp.float32)
    value_sum = jnp.einsum(
        "ds,df->sf", normed_full, expand_value, preferred_element_type=jnp.float32
    )
    rms_mid = lax.rsqrt(mid_squares / width + epsilon)
    act = (jax.nn.silu(rms_mid[:, None] * gate_sum) * (rms_mid[:, None] * value_sum)).astype(
        jnp.bfloat16
    )
    columns = reduce_proj
    channel = lax.psum_scatter(
        jnp.einsum("fd,sf->ds", columns, act, preferred_element_type=jnp.float32),
        ("kv", "tp"),
        scatter_dimension=0,
        tiled=True,
    )
    return (mid.astype(jnp.float32) + channel).astype(jnp.bfloat16)


def solution(mesh):
    return jax.shard_map(
        shards,
        mesh=mesh,
        in_specs=(
            P(("kv", "tp"), "dp"),
            P(),
            P(None, "kv", "tp"),
            P(None, "kv", "tp"),
            P(None, "kv"),
            P(None, "kv"),
            P(),
            P(),
            P(),
            P(),
            P(None, None, "tp"),
            P(),
            P(),
            P(("dp", "kv"), None, None, "tp"),
            P(("dp", "kv"), None, None),
            P(("dp", "kv"), None, None),
            P(("dp", "kv"), None, "tp", None),
            P(("dp", "kv"), None, None, "tp"),
            P(("dp", "kv"), None, None),
            P(("dp", "kv"), None, None),
            P(("dp", "kv")),
            P(None, "tp"),
            P("kv", "tp", None),
            P(),
            P(None, ("kv", "tp")),
            P(None, ("kv", "tp")),
            P(("kv", "tp"), None),
        ),
        out_specs=P(("kv", "tp"), "dp"),
        check_vma=False,
    )
```

profile of v0, /device:TPU:0, one launch (start us, length us, event | category | flops | bytes accessed | tf_op | source)
XLA Modules:
  0.0 156.3 jit_solution(15144254045306652727)
XLA Ops:
  6.5 14.7 %all_gather.3 = bf16[2048,4]{0,1:T(4,128)(2,1)S(1)} all-gather(bf16[256,4]{0,1:T(4,128)(2,1)} %param.27), channel_id=1, replica_groups=mesh['dp'=4,'kv'=4,'tp'=2] {'kv','tp'}, dimensions={0}, use_global_device_ids=true | all-gather | bytes 18432 | tf_op jit(solution)/shard_map/all_gather | solution.py:59
  21.3 0.8 fusion.15
  22.1 1.4 fusion.7
  25.4 3.4 %all-to-all-start = ((bf16[4,2,128]{2,1,0:T(2,128)(2,1)}), bf16[4,2,128]{2,1,0:T(2,128)(2,1)S(1)}, u32[]{:S(2)}, u32[]{:S(2)}) async-start(bf16[4,2,128]{2,1,0:T(2,128)(2,1)} %reshape.385), calls=%async_computation | async-start | bytes 4096 | tf_op jit(solution)/shard_map/all_to_all | solution.py:89
  29.5 1.4 fusion.6
  31.0 3.1 %fusion.1 = bf16[4,16,32]{2,0,1:T(4,128)(2,1)S(1)} fusion(bf16[2048,16,32]{0,2,1:T(8,128)(2,1)} %param.29, bf16[2048,4]{0,1:T(4,128)(2,1)S(1)} %get-tuple-element.16, f32[4]{0:T(128)S(1)} %add_rsqrt_fusion.2), kind=kOutput, calls=%fused_computation.5 | convolution fusion | flops 8392704 | bytes 2117648 | tf_op jit(solution)/shard_map/ds,dhp->shp/dot_general | solution.py:65
  34.1 1.5 fusion
  36.9 5.1 %all-to-all-start.1 = ((bf16[4,2,128]{2,1,0:T(2,128)(2,1)}), bf16[4,2,128]{2,1,0:T(2,128)(2,1)S(1)}, u32[]{:S(2)}, u32[]{:S(2)}) async-start(bf16[4,2,128]{2,1,0:T(2,128)(2,1)} %reshape.387), calls=%async_computation.1 | async-start | bytes 4096 | tf_op jit(solution)/shard_map/all_to_all | solution.py:88
  43.3 0.7 reshape.381
  44.0 0.7 reshape.383
  45.0 2.5 %all-to-all-done.1 = bf16[4,2,128]{2,1,0:T(2,128)(2,1)S(1)} async-done(((bf16[4,2,128]{2,1,0:T(2,128)(2,1)}), bf16[4,2,128]{2,1,0:T(2,128)(2,1)S(1)}, u32[]{:S(2)}, u32[]{:S(2)}) %all-to-all-start.1) | async-done | bytes 2080 | tf_op jit(solution)/shard_map/all_to_all | solution.py:88
  47.5 3.2 %all-to-all-start.2 = ((bf16[4,2,256]{2,1,0:T(2,128)(2,1)}), bf16[4,2,256]{2,1,0:T(2,128)(2,1)S(1)}, u32[]{:S(2)}, u32[]{:S(2)}) async-start(bf16[4,2,256]{2,1,0:T(2,128)(2,1)} %reshape.383), calls=%async_computation.2 | async-start | bytes 8192 | tf_op jit(solution)/shard_map/all_to_all | solution.py:87
  50.8 0.8 multiply_reduce_fusion.3
  52.2 3.4 %fusion.43 = f32[8,1,8,32]{3,1,2,0:T(1,128)S(1)} fusion(f32[8,8,32,128]{3,2,1,0:T(8,128)} %bitcast.136, bf16[8,128,1,1]{1,0,2,3:T(8,128)(2,1)S(1)} %get-tuple-element.17), kind=kOutput, calls=%fused_computation.72 | convolution fusion | flops 3145728 | bytes 1058816 | tf_op jit(solution)/shard_map/sgn,sgrpn->sgrp/dot_general | solution.py:120
  55.6 1.8 %fusion.57 = (f32[64]{0:T(128)S(1)}, f32[64]{0:T(128)S(1)}, f32[64]{0:T(128)S(1)}) fusion(f32[64]{0:T(128)} %get-tuple-element.13, f32[64]{0:T(128)} %param.35, f32[64]{0:T(128)S(1)} %broadcast_in_dim.11, f32[64]{0:T(128)} %param.34, bf16[2048,64]{0,1:T(8,128)(2,1)} %param.33, bf16[2048,4]{0,1:T(4,128)(2,1)S(1)} %get-tuple-element.16, s32[]{:T(128)S(6)} %select_n.13, ...), kind=kOutput, calls=%fused_computation.90 | convolution fusion | flops 263040 | bytes 272392 | tf_op jit(solution)/shard_map/ds,dh->sh/dot_general | solution.py:83
  57.4 0.8 fusion.19
  58.2 5.1 %all-to-all-start.3 = ((bf16[4,2,256]{2,1,0:T(2,128)(2,1)}), bf16[4,2,256]{2,1,0:T(2,128)(2,1)S(1)}, u32[]{:S(2)}, u32[]{:S(2)}) async-start(bf16[4,2,256]{2,1,0:T(2,128)(2,1)} %reshape.381), calls=%async_computation.3 | async-start | bytes 8192 | tf_op jit(solution)/shard_map/all_to_all | solution.py:86
  63.3 1.4 multiply_reduce_fusion
  65.0 3.9 %all-to-all-done.3 = bf16[4,2,256]{2,1,0:T(2,128)(2,1)S(1)} async-done(((bf16[4,2,256]{2,1,0:T(2,128)(2,1)}), bf16[4,2,256]{2,1,0:T(2,128)(2,1)S(1)}, u32[]{:S(2)}, u32[]{:S(2)}) %all-to-all-start.3) | async-done | bytes 4128 | tf_op jit(solution)/shard_map/all_to_all | solution.py:86
  69.0 1.3 multiply_reduce_fusion.2
  70.5 0.7 reduce.14
  71.2 0.7 reshape.389
  71.9 3.2 %all-to-all-start.4 = ((bf16[4,2,256]{2,1,0:T(2,128)(2,1)}), bf16[4,2,256]{2,1,0:T(2,128)(2,1)S(1)}, u32[]{:S(2)}, u32[]{:S(2)}) async-start(bf16[4,2,256]{2,1,0:T(2,128)(2,1)} %reshape.389), calls=%async_computation.4 | async-start | bytes 8192 | tf_op jit(solution)/shard_map/all_to_all | solution.py:140
  75.2 0.8 dynamic_update_slice.3
  75.9 4.7 %all-to-all-done.4 = bf16[4,2,256]{2,1,0:T(2,128)(2,1)S(1)} async-done(((bf16[4,2,256]{2,1,0:T(2,128)(2,1)}), bf16[4,2,256]{2,1,0:T(2,128)(2,1)S(1)}, u32[]{:S(2)}, u32[]{:S(2)}) %all-to-all-start.4) | async-done | bytes 4128 | tf_op jit(solution)/shard_map/all_to_all | solution.py:140
  80.8 2.0 %convolution_bitcast_fusion.1 = f32[2048,4]{0,1:T(4,128)S(1)} fusion(bf16[16,32,2048]{2,1,0:T(8,128)(2,1)} %param.49, bf16[4,16,32]{2,1,0:T(8,128)(2,1)S(1)} %bitcast.141), kind=kOutput, calls=%fused_computation.1 | convolution fusion | flops 8388608 | bytes 2134016 | tf_op jit(solution)/shard_map/hpd,shp->ds/dot_general | solution.py:143
  82.8 26.3 %all-reduce = (f32[2048,4]{0,1:T(4,128)S(1)}, f32[4]{0:T(128)S(1)}) all-reduce(f32[2048,4]{0,1:T(4,128)S(1)} %convolution_bitcast_fusion.1, f32[4]{0:T(128)S(1)} %dynamic_update_slice.3), channel_id=1, replica_groups=mesh['dp'=4,'kv'=4,'tp'=2] {'kv','tp'}, use_global_device_ids=true, to_apply=%region_9.10 | all-reduce | flops 8196 | bytes 65568 | tf_op jit(solution)/shard_map/psum | solution.py:142
  109.3 2.7 %convolution_multiply_fusion.3 = f32[4,704]{1,0:T(4,128)S(1)} fusion(bf16[2048,704]{0,1:T(8,128)(2,1)} %param.51, bf16[2048,4]{0,1:T(4,128)(2,1)S(1)} %get-tuple-element.8, f32[2048]{0:T(1024)S(1)} %copy-done.4, f32[4]{0:T(128)S(1)} %add_rsqrt_fusion), kind=kOutput, calls=%fused_computation.8 | convolution fusion | flops 11561728 | bytes 2919440 | tf_op jit(solution)/shard_map/ds,df->sf/dot_general | solution.py:151
  112.0 3.5 %convolution_bitcast_fusion = f32[2048,4]{0,1:T(4,128)S(1)} fusion(bf16[704,2048]{1,0:T(8,128)(2,1)S(1)} %copy-done, bf16[2048,704]{0,1:T(8,128)(2,1)} %param.52, f32[4,704]{1,0:T(4,128)S(1)} %convolution_multiply_fusion.3, bf16[2048,4]{0,1:T(4,128)(2,1)S(1)} %get-tuple-element.8, f32[2048]{0:T(1024)S(1)} %copy-done.4, f32[4]{0:T(128)S(1)} %add_rsqrt_fusion), kind=kOutput, calls=%fused_computation | convolution fusion | flops 23112960 | bytes 5835792 | tf_op jit(solution)/shard_map/fd,sf->ds/dot_general | solution.py:161
  115.5 1.4 copy.71
  116.9 31.0 %reduce-scatter.4.cloned.1.call-done = f32[256,4]{1,0:T(8,128)} async-done(((f32[2048,4]{1,0:T(8,128)}), f32[256,4]{1,0:T(8,128)}) %reduce-scatter.4.cloned.1.call-update) | async-done | bytes 4112
  147.8 1.0 copy.72
  (63 shorter events, 7.1 us)
Async XLA Ops:
  6.5 105.4 %copy-start = (bf16[704,2048]{1,0:T(8,128)(2,1)S(1)}, bf16[704,2048]{1,0:T(8,128)(2,1)}, u32[]{:S(2)}) copy-start(bf16[704,2048]{1,0:T(8,128)(2,1)} %param.53) | copy-start | bytes 8650756
  23.5 13.3 %copy-start.5 = (f32[1,128,64]{1,2,0:T(8,128)S(1)}, f32[1,128,64]{1,2,0:T(8,128)}, u32[]{:S(2)}) copy-start(f32[1,128,64]{1,2,0:T(8,128)} %param.46) | copy-start | bytes 98308
  23.5 21.1 %copy-start.2 = (bf16[1,128,1024]{2,1,0:T(8,128)(2,1)S(1)}, bf16[1,128,1024]{2,1,0:T(8,128)(2,1)}, u32[]{:S(2)}) copy-start(bf16[1,128,1024]{2,1,0:T(8,128)(2,1)} %param.45) | copy-start | bytes 786436
  25.4 11.5 %all-to-all-start = ((bf16[4,2,128]{2,1,0:T(2,128)(2,1)}), bf16[4,2,128]{2,1,0:T(2,128)(2,1)S(1)}, u32[]{:S(2)}, u32[]{:S(2)}) async-start(bf16[4,2,128]{2,1,0:T(2,128)(2,1)} %reshape.385), calls=%async_computation | async-start | bytes 4096 | tf_op jit(solution)/shard_map/all_to_all | solution.py:89
  28.7 5.3 %copy-start.1 = (bf16[2048,16,32]{0,2,1:T(8,128)(2,1)S(1)}, bf16[2048,16,32]{0,2,1:T(8,128)(2,1)}, u32[]{:S(2)}) copy-start(bf16[2048,16,32]{0,2,1:T(8,128)(2,1)} %param.30) | copy-start | bytes 6291460
  34.1 34.9 %copy-start.6 = (bf16[1,3,64,32]{2,3,1,0:T(8,128)(2,1)S(1)}, bf16[1,3,64,32]{2,3,1,0:T(8,128)(2,1)}, u32[]{:S(2)}) copy-start(bf16[1,3,64,32]{2,3,1,0:T(8,128)(2,1)} %param.40) | copy-start | bytes 36868
  34.1 36.2 %copy-start.7 = (f32[64,32]{0,1:T(8,128)S(1)}, f32[64,32]{0,1:T(8,128)}, u32[]{:S(2)}) copy-start(f32[64,32]{0,1:T(8,128)} %param.48) | copy-start | bytes 24580
  35.6 8.4 %copy-start.8 = (f32[128]{0:T(128)}, f32[128]{0:T(128)S(1)}, u32[]{:S(2)}) copy-start(f32[128]{0:T(128)S(1)} %compare_convert_fusion) | copy-start | bytes 1540
  36.9 10.6 %all-to-all-start.1 = ((bf16[4,2,128]{2,1,0:T(2,128)(2,1)}), bf16[4,2,128]{2,1,0:T(2,128)(2,1)S(1)}, u32[]{:S(2)}, u32[]{:S(2)}) async-start(bf16[4,2,128]{2,1,0:T(2,128)(2,1)} %reshape.387), calls=%async_computation.1 | async-start | bytes 4096 | tf_op jit(solution)/shard_map/all_to_all | solution.py:88
  44.8 24.2 %copy-start.3 = (f32[4,64,32]{1,2,0:T(8,128)S(1)}, f32[4,64,32]{1,2,0:T(8,128)}, u32[]{:S(2)}) copy-start(f32[4,64,32]{1,2,0:T(8,128)} %param.37) | copy-start | bytes 98308
  47.5 10.7 %all-to-all-start.2 = ((bf16[4,2,256]{2,1,0:T(2,128)(2,1)}), bf16[4,2,256]{2,1,0:T(2,128)(2,1)S(1)}, u32[]{:S(2)}, u32[]{:S(2)}) async-start(bf16[4,2,256]{2,1,0:T(2,128)(2,1)} %reshape.383), calls=%async_computation.2 | async-start | bytes 8192 | tf_op jit(solution)/shard_map/all_to_all | solution.py:87
  50.8 58.5 %copy-start.4 = (f32[2048]{0:T(1024)S(1)}, f32[2048]{0:T(1024)}, u32[]{:S(2)}) copy-start(f32[2048]{0:T(1024)} %param.50) | copy-start | bytes 24580
  58.2 10.6 %all-to-all-start.3 = ((bf16[4,2,256]{2,1,0:T(2,128)(2,1)}), bf16[4,2,256]{2,1,0:T(2,128)(2,1)S(1)}, u32[]{:S(2)}, u32[]{:S(2)}) async-start(bf16[4,2,256]{2,1,0:T(2,128)(2,1)} %reshape.381), calls=%async_computation.3 | async-start | bytes 8192 | tf_op jit(solution)/shard_map/all_to_all | solution.py:86
  71.9 8.8 %all-to-all-start.4 = ((bf16[4,2,256]{2,1,0:T(2,128)(2,1)}), bf16[4,2,256]{2,1,0:T(2,128)(2,1)S(1)}, u32[]{:S(2)}, u32[]{:S(2)}) async-start(bf16[4,2,256]{2,1,0:T(2,128)(2,1)} %reshape.389), calls=%async_computation.4 | async-start | bytes 8192 | tf_op jit(solution)/shard_map/all_to_all | solution.py:140
  75.1 72.7 %reduce-scatter.4.cloned.1.call-start = ((), (), s32[]{:S(2)}) async-start(), calls=%async_computation.6 | async-start | bytes 1179648
Sparse Core Ops, SparseCore 0:
  117.0 30.8 reduce-scatter.3
where the time goes:
time: 157 us; the launch traced here: 156 us
  waiting for transfers between devices  42.1 us (27%)
  blocking collectives  41 us (26%)
  matrix products  20.9 us (13%)
  starting transfers between devices  20 us (13%)
  between operations  14.4 us (9%)
  other arithmetic  8.9 us (6%)
  local copies, waits for them, and re-layouts  8.85 us (6%)
    unnamed x2, waiting for transfers between devices  31 us
    psum x1, blocking collectives, shards(): lax.psum(jnp.einsum('hpd,shp->ds', columns, by_head, preferred_element_ty...  26.3 us
    all_gather x1, blocking collectives, shards(): whole_rows = lax.all_gather(hidden, ('kv', 'tp'), axis=0, tiled=True)  14.7 us
    unnamed x33, local copies, waits for them, and re-layouts  6.14 us
    all_to_all x1, starting transfers between devices, shards(): lax.all_to_all(input_part, 'kv', split_axis=0, concat_axis=1, tiled=True)  5.1 us
    all_to_all x1, starting transfers between devices, shards(): lax.all_to_all(gate_part, 'kv', split_axis=0, concat_axis=1, tiled=True)  5.06 us
    all_to_all x1, waiting for transfers between devices, shards(): lax.all_to_all(gated, 'kv', split_axis=1, concat_axis=0, tiled=True)  4.73 us
    all_to_all x1, waiting for transfers between devices, shards(): lax.all_to_all(gate_part, 'kv', split_axis=0, concat_axis=1, tiled=True)  3.87 us
  transfers between devices with their start and end apart: 6, of which 4 were waited for; matrix products, arithmetic and copies ran while one was open for 13% of the time, Pallas kernels for 0%

commit v1 on v0

--- a/solution.py
+++ b/solution.py
@@ -2,6 +2,9 @@
 import jax.numpy as jnp
 from jax import lax
 from jax.sharding import PartitionSpec as P
+from jax.experimental import pallas as pl
+from jax.experimental.pallas import tpu as pltpu
+import functools
 
 MIXER_HEADS = 64
 HEAD_DIM = 64
@@ -166,9 +169,480 @@
     return (mid.astype(jnp.float32) + channel).astype(jnp.bfloat16)
 
 
+MESH = pl.DeviceIdType.MESH
+HIGHEST = lax.Precision.HIGHEST
+F32 = jnp.float32
+BF16 = jnp.bfloat16
+
+
+def silu(v):
+    return v / (1.0 + jnp.exp(-v))
+
+
+def rounded(v):
+    return v.astype(BF16).astype(F32)
+
+
+def matmul(a, b):
+    return lax.dot_general(a, b, (((1,), (0,)), ((), ())), preferred_element_type=F32)
+
+
+def matmul_t(a, b):
+    return lax.dot_general(a, b, (((1,), (1,)), ((), ())), preferred_element_type=F32)
+
+
+def matmul_exact(a, b):
+    return lax.dot_general(
+        a, b, (((1,), (0,)), ((), ())), precision=HIGHEST, preferred_element_type=F32
+    )
+
+
+def layer_kernel(
+    kv_n,
+    tp_n,
+    lengths,
+    hidden,
+    mixer_gain,
+    step_bias,
+    decay_log,
+    skip_gain,
+    taps_inner,
+    taps_input,
+    taps_output,
+    recent_inner,
+    recent_input,
+    recent_output,
+    block_decay,
+    norm_gain,
+    channel_gain,
+    gate_hbm,
+    inner_hbm,
+    input_hbm,
+    output_hbm,
+    step_hbm,
+    block_input_hbm,
+    states_hbm,
+    block_inner_hbm,
+    mixer_out_hbm,
+    expand_gate_hbm,
+    expand_value_hbm,
+    reduce_hbm,
+    out,
+    gate_w,
+    inner_w,
+    input_w,
+    output_w,
+    step_w,
+    block_input,
+    states,
+    block_inner,
+    mixer_out,
+    expand_gate,
+    expand_value,
+    reduce_w,
+    head_mask,
+    hid_all,
+    pre_send,
+    pre_recv,
+    gated_send,
+    gated_recv,
+    part_send,
+    part_recv,
+    mid_send,
+    mid_recv,
+    last_send,
+    last_recv,
+    load_sem,
+    send_sem,
+    recv_sem,
+):
+    n = kv_n * tp_n
+    kv = lax.axis_index("kv")
+    tp = lax.axis_index("tp")
+    me = kv * tp_n + tp
+    seqs, rows = hidden.shape
+    half, heads = norm_gain.shape
+    groups_n = input_w.shape[1] * kv_n
+    state = states.shape[1]
+    groups = groups_n // state
+    per_group = heads // groups
+    span = block_decay.shape[1]
+    channels = heads * half
+    own_ch = channels // kv_n
+    own_in = input_w.shape[1]
+
+    pairs = (
+        (output_hbm, output_w),
+        (input_hbm, input_w),
+        (inner_hbm, inner_w),
+        (gate_hbm, gate_w),
+        (step_hbm, step_w),
+        (block_input_hbm, block_input),
+        (states_hbm, states),
+        (block_inner_hbm, block_inner),
+        (mixer_out_hbm, mixer_out),
+        (expand_gate_hbm, expand_gate),
+        (expand_value_hbm, expand_value),
+        (reduce_hbm, reduce_w),
+    )
+    loads = {}
+    for i, (src, dst) in enumerate(pairs):
+        copy = pltpu.make_async_copy(src, dst, load_sem.at[i])
+        copy.start()
+        loads[id(dst)] = copy
+
+    def loaded(ref):
+        loads[id(ref)].wait()
+        return ref[...]
+
+    def peer(k):
+        other = lax.rem(me + k, n)
+        return other, {"kv": other // tp_n, "tp": lax.rem(other, tp_n)}
+
+    barrier = pltpu.get_barrier_semaphore()
+    for k in range(1, n):
+        pl.semaphore_signal(barrier, inc=1, device_id=peer(k)[1], device_id_type=MESH)
+    pl.semaphore_wait(barrier, n - 1)
+
+    pending = []
+
+    def to_all(phase, src_of, dst):
+        copies = []
+        for k in range(1, n):
+            other, where = peer(k)
+            copy = pltpu.make_async_remote_copy(
+                src_ref=src_of(other),
+                dst_ref=dst.at[me],
+                send_sem=send_sem.at[phase * n + k],
+                recv_sem=recv_sem.at[phase * n + k],
+                device_id=where,
+                device_id_type=MESH,
+            )
+            copy.start()
+            copies.append(copy)
+        pending.extend(copies)
+        return copies
+
+    def to_line(phase, src, dst):
+        copies = []
+        for k in range(1, kv_n):
+            other = lax.rem(kv + k, kv_n)
+            copy = pltpu.make_async_remote_copy(
+                src_ref=src.at[other],
+                dst_ref=dst.at[kv],
+                send_sem=send_sem.at[phase * n + k],
+                recv_sem=recv_sem.at[phase * n + k],
+                device_id={"kv": other},
+                device_id_type=MESH,
+            )
+            copy.start()
+            copies.append(copy)
+        pending.extend(copies)
+        return copies
+
+    gather = to_all(0, lambda other: hidden, hid_all)
+    hid_all[me] = hidden[...]
+
+    column = lax.broadcasted_iota(jnp.int32, (heads, channels), 1)
+    row = lax.broadcasted_iota(jnp.int32, (heads, channels), 0)
+    head_mask[...] = jnp.where(
+        (column >= row * half) & (column < (row + 1) * half), 1.0, 0.0
+    )
+    lane = lax.broadcasted_iota(jnp.int32, (half, channels), 1)
+    channel = lax.broadcasted_iota(jnp.int32, (half, channels), 0)
+    pick = jnp.where(jnp.bitwise_and(lane, half - 1) == channel, 1.0, 0.0)
+    window = taps_inner[0] * recent_inner[0].astype(F32)
+    for t in range(1, recent_inner.shape[0]):
+        window = window + taps_inner[t] * recent_inner[t].astype(F32)
+    last = taps_inner.shape[0] - 1
+
+    def spread(a):
+        return jnp.sum(pick * matmul_exact(a, head_mask[...]), axis=0, keepdims=True)
+
+    window_row = spread(window)
+    tap_row = spread(taps_inner[last])
+    norm_row = spread(norm_gain[...])
+
+    def past(taps, recent):
+        total = taps[0:1, :] * recent[0:1, :].astype(F32)
+        for t in range(1, recent.shape[0]):
+            total = total + taps[t : t + 1, :] * recent[t : t + 1, :].astype(F32)
+        return total
+
+    past_input = past(taps_input, recent_input)
+    past_output = past(taps_output, recent_output)
+    diagonal = lax.broadcasted_iota(jnp.int32, (heads, heads), 0) == lax.broadcasted_iota(
+        jnp.int32, (heads, heads), 1
+    )
+
+    def as_column(v):
+        return jnp.sum(jnp.where(diagonal, v, 0.0), axis=1, keepdims=True)
+
+    bias = as_column(step_bias[...])
+    rate = jnp.exp(as_column(decay_log[...]))
+    skip = as_column(skip_gain[...])
+    position = lax.broadcasted_iota(jnp.int32, (1, span), 1)
+    live = jnp.where(position < lengths[0], 1.0, 0.0)
+    masked = block_decay[...] * live
+    cached = jnp.sum(masked, axis=1, keepdims=True)
+    later = jnp.where(
+        lax.broadcasted_iota(jnp.int32, (span, span), 0)
+        > lax.broadcasted_iota(jnp.int32, (span, span), 1),
+        1.0,
+        0.0,
+    )
+    suffix = matmul_exact(masked, later)
+
+    for copy in gather:
+        copy.wait_recv()
+    whole = jnp.concatenate([hid_all[i].astype(F32) for i in range(n)], axis=1)
+    rms_in = lax.rsqrt(jnp.mean(whole * whole, axis=1, keepdims=True) + epsilon)
+    normed = (whole * mixer_gain[...]).astype(BF16)
+    output_part = rounded(rms_in * matmul(normed, loaded(output_w)))
+    input_part = rounded(rms_in * matmul(normed, loaded(input_w)))
+    inner_part = rounded(rms_in * matmul_t(normed, loaded(inner_w)))
+    gate_part = rounded(rms_in * matmul_t(normed, loaded(gate_w)))
+    bounds = (0, own_in, 2 * own_in, 2 * own_in + own_ch, 2 * own_in + 2 * own_ch)
+    parts = (output_part, input_part, inner_part, gate_part)
+    for s in range(seqs):
+        for i in range(4):
+            pre_send[s, :, bounds[i] : bounds[i + 1]] = parts[i][s : s + 1, :]
+    exchange = to_line(1, pre_send, pre_recv)
+    pre_recv[kv] = pre_send[kv]
+
+    mine = lax.broadcasted_iota(jnp.int32, (seqs, 1), 0) == kv
+    own_rms = jnp.sum(jnp.where(mine, rms_in, 0.0), axis=0, keepdims=True)
+    step_all = matmul_t(loaded(step_w), normed)
+    mine_lane = lax.broadcasted_iota(jnp.int32, (heads, seqs), 1) == kv
+    step_pre = rounded(
+        own_rms * jnp.sum(jnp.where(mine_lane, step_all, 0.0), axis=1, keepdims=True)
+    )
+    v = step_pre + bias
+    step = jnp.maximum(v, 0.0) + jnp.log1p(jnp.exp(-jnp.abs(v)))
+    new_decay = -rate * step
+    kept = live * jnp.exp(new_decay + suffix)
+    total = jnp.exp(new_decay + cached)
+    states_b = loaded(states).astype(BF16)
+
+    for copy in exchange:
+        copy.wait_recv()
+
+    def gathered(i):
+        return jnp.concatenate(
+            [pre_recv[s, :, bounds[i] : bounds[i + 1]] for s in range(kv_n)], axis=1
+        )
+
+    conv_output = rounded(silu(past_output + taps_output[last : last + 1, :] * gathered(0)))
+    conv_input = silu(past_input + taps_input[last : last + 1, :] * gathered(1))
+
+    def by_head(v):
+        return jnp.concatenate(
+            [
+                jnp.broadcast_to(v[:, g * state : (g + 1) * state], (per_group, state))
+                for g in range(groups)
+            ],
+            axis=0,
+        )
+
+    readout = by_head(conv_output)
+    readout_b = readout.astype(BF16)
+    own_score = jnp.sum(readout * by_head(conv_input), axis=1, keepdims=True)
+    block_in = loaded(block_input)
+    score = jnp.concatenate(
+        [
+            matmul_t(
+                readout_b[g * per_group : (g + 1) * per_group, :],
+                block_in[:, g * state : (g + 1) * state],
+            )
+            for g in range(groups)
+        ],
+        axis=0,
+    )
+    weight = (kept * score).astype(BF16)
+    cross = matmul_t(weight, loaded(block_inner)) + total * matmul_t(readout_b, states_b)
+    mask = head_mask[...]
+    direct = jnp.sum(mask * (own_score * step + skip), axis=0, keepdims=True)
+    conv_inner = silu(window_row + tap_row * gathered(2))
+    mix = jnp.sum(mask * cross, axis=0, keepdims=True) + direct * conv_inner
+    gated_raw = mix * silu(gathered(3))
+    squares = jnp.sum(gated_raw * gated_raw, axis=1, keepdims=True)
+    gated = rounded(gated_raw * norm_row)
+    tail = gated_send.shape[2] - own_ch
+    for s in range(kv_n):
+        gated_send[s, :, :own_ch] = gated[:, s * own_ch : (s + 1) * own_ch]
+        gated_send[s, :, own_ch:] = jnp.broadcast_to(squares, (1, tail))
+    heads_out = to_line(2, gated_send, gated_recv)
+    gated_recv[kv] = gated_send[kv]
+    out_w = loaded(mixer_out)
+    for copy in heads_out:
+        copy.wait_recv()
+    received = jnp.concatenate([gated_recv[s] for s in range(kv_n)], axis=0)
+    partial = matmul(received[:, :own_ch].astype(BF16), out_w)
+    for i in range(n):
+        part_send[i, :, :rows] = partial[:, i * rows : (i + 1) * rows]
+        part_send[i, :, rows:] = received[:, own_ch:]
+    reduce_mid = to_all(3, lambda other: part_send.at[other], part_recv)
+    part_recv[me] = part_send[me]
+    own_hidden = hidden[...].astype(F32)
+    for copy in reduce_mid:
+        copy.wait_recv()
+    summed = part_recv[0]
+    for i in range(1, n):
+        summed = summed + part_recv[i]
+    gate_squares = summed[:, rows : rows + 1] / kv_n
+    rms_gate = lax.rsqrt(gate_squares / (channels * tp_n) + epsilon)
+    mid = rounded(own_hidden + rms_gate * summed[:, :rows])
+    mid_send[...] = mid
+    gather_mid = to_all(4, lambda other: mid_send, mid_recv)
+    mid_recv[me] = mid
+    for copy in gather_mid:
+        copy.wait_recv()
+    full = jnp.concatenate([mid_recv[i] for i in range(n)], axis=1)
+    rms_mid = lax.rsqrt(jnp.mean(full * full, axis=1, keepdims=True) + epsilon)
+    normed_mid = (full * channel_gain[...]).astype(BF16)
+    gate_sum = rms_mid * matmul_t(normed_mid, loaded(expand_gate))
+    value_sum = rms_mid * matmul_t(normed_mid, loaded(expand_value))
+    act = (silu(gate_sum) * value_sum).astype(BF16)
+    down = matmul(act, loaded(reduce_w))
+    for i in range(n):
+        last_send[i] = down[:, i * rows : (i + 1) * rows]
+    final = to_all(5, lambda other: last_send.at[other], last_recv)
+    last_recv[me] = last_send[me]
+    for copy in final:
+        copy.wait_recv()
+    added = last_recv[0]
+    for i in range(1, n):
+        added = added + last_recv[i]
+    out[...] = (mid + added).astype(out.dtype)
+    for copy in pending:
+        copy.wait_send()
+
+
+def fused(
+    kv_n,
+    tp_n,
+    hidden,
+    mixer_gain,
+    gate_proj,
+    inner_proj,
+    input_proj,
+    output_proj,
+    step_proj,
+    step_bias,
+    decay_log,
+    skip_gain,
+    taps_inner,
+    taps_input,
+    taps_output,
+    recent_inner,
+    recent_input,
+    recent_output,
+    states,
+    block_inner,
+    block_input,
+    block_decay,
+    lengths,
+    norm_gain,
+    mixer_out,
+    channel_gain,
+    expand_gate,
+    expand_value,
+    reduce_proj,
+):
+    rows, seqs = hidden.shape
+    width = reduce_proj.shape[1]
+    _, heads, half, state = states.shape
+    channels = heads * half
+    n = kv_n * tp_n
+    own_ch = channels // kv_n
+    own_in = input_proj.shape[1]
+    small = (
+        hidden.T,
+        mixer_gain[None],
+        step_bias[None],
+        decay_log[None],
+        skip_gain[None],
+        taps_inner.transpose(0, 2, 1),
+        taps_input,
+        taps_output,
+        recent_inner[0].transpose(0, 2, 1),
+        recent_input[0],
+        recent_output[0],
+        block_decay[0].T,
+        norm_gain.T,
+        channel_gain[None],
+    )
+    large = (
+        gate_proj.transpose(1, 2, 0).reshape(own_ch, width),
+        inner_proj.transpose(1, 2, 0).reshape(own_ch, width),
+        input_proj,
+        output_proj,
+        step_proj.T,
+        block_input[0],
+        states.reshape(channels, state),
+        block_inner[0].transpose(1, 2, 0).reshape(channels, -1),
+        mixer_out.reshape(own_ch, width),
+        expand_gate.T,
+        expand_value.T,
+        reduce_proj,
+    )
+    pre = 2 * own_in + 2 * own_ch
+    result = pl.pallas_call(
+        functools.partial(layer_kernel, kv_n, tp_n),
+        out_shape=jax.ShapeDtypeStruct((seqs, rows), hidden.dtype),
+        in_specs=[pl.BlockSpec(memory_space=pltpu.SMEM)]
+        + [pl.BlockSpec(memory_space=pltpu.VMEM)] * len(small)
+        + [pl.BlockSpec(memory_space=pl.ANY)] * len(large),
+        out_specs=pl.BlockSpec(memory_space=pltpu.VMEM),
+        scratch_shapes=[pltpu.VMEM(a.shape, a.dtype) for a in large]
+        + [
+            pltpu.VMEM((heads, channels), F32),
+            pltpu.VMEM((n, seqs, rows), hidden.dtype),
+            pltpu.VMEM((kv_n, 1, pre), F32),
+            pltpu.VMEM((kv_n, 1, pre), F32),
+            pltpu.VMEM((kv_n, 1, own_ch + 128), F32),
+            pltpu.VMEM((kv_n, 1, own_ch + 128), F32),
+            pltpu.VMEM((n, seqs, rows + 128), F32),
+            pltpu.VMEM((n, seqs, rows + 128), F32),
+            pltpu.VMEM((seqs, rows), F32),
+            pltpu.VMEM((n, seqs, rows), F32),
+            pltpu.VMEM((n, seqs, rows), F32),
+            pltpu.VMEM((n, seqs, rows), F32),
+            pltpu.SemaphoreType.DMA((len(large),)),
+            pltpu.SemaphoreType.DMA((6 * n,)),
+            pltpu.SemaphoreType.DMA((6 * n,)),
+        ],
+        compiler_params=pltpu.CompilerParams(
+            collective_id=0, has_side_effects=True, vmem_limit_bytes=56 * 1024 * 1024
+        ),
+    )(lengths, *small, *large)
+    return result.T
+
+
+def wide_enough(kv_n, tp_n, args):
+    hidden, input_proj, states = args[0], args[4], args[16]
+    rows = hidden.shape[0]
+    seq_dev, heads, half, state = states.shape
+    return (
+        seq_dev == 1
+        and hidden.shape[1] == kv_n
+        and rows % 128 == 0
+        and (heads * half) % (kv_n * 128) == 0
+        and input_proj.shape[1] % 128 == 0
+        and half & (half - 1) == 0
+        and state % 128 == 0
+    )
+
+
+def layer(kv_n, tp_n, *args):
+    if wide_enough(kv_n, tp_n, args):
+        return fused(kv_n, tp_n, *args)
+    return shards(*args)
+
+
 def solution(mesh):
     return jax.shard_map(
-        shards,
+        functools.partial(layer, mesh.shape["kv"], mesh.shape["tp"]),
         mesh=mesh,
         in_specs=(
             P(("kv", "tp"), "dp"),

time: 157 us -> 37.5 us (0.24)
  waiting for transfers between devices: 42.1 us -> 0 us
  blocking collectives: 41 us -> 0 us
  Pallas kernels: 0 us -> 35.3 us
  matrix products: 20.9 us -> 0 us
  starting transfers between devices: 20 us -> 0 us
  between operations: 14.4 us -> 0.66 us
  other arithmetic: 8.9 us -> 0 us
  local copies, waits for them, and re-layouts: 8.85 us -> 1.26 us
    pallas_call x0 -> x1, Pallas kernels: none -> 35.3 us  [fused(): pl.pallas_call(functools.partial(layer_kernel, kv_n, tp_n), out_shape=jax...]
    unnamed x2 -> x0, waiting for transfers between devices: 31 us -> none
    psum x1 -> x0, blocking collectives: 26.3 us -> none  [shards(): lax.psum(jnp.einsum('hpd,shp->ds', columns, by_head, preferred_element_ty...]
    dot_general x10 -> x0, matrix products: 20.9 us -> none  [the longest x1 3.49 us: shards(): jnp.einsum('fd,sf->ds', columns, act, preferred_element_type=jnp.float32)]
    all_to_all x5 -> x0, starting transfers between devices: 20 us -> none  [the longest x1 5.1 us: shards(): lax.all_to_all(input_part, 'kv', split_axis=0, concat_axis=1, tiled=True)]
    all_gather x1 -> x0, blocking collectives: 14.7 us -> none  [shards(): whole_rows = lax.all_gather(hidden, ('kv', 'tp'), axis=0, tiled=True)]
    all_to_all x5 -> x0, waiting for transfers between devices: 11.1 us -> none  [the longest x1 4.73 us: shards(): lax.all_to_all(gated, 'kv', split_axis=1, concat_axis=0, tiled=True)]
    unnamed x33 -> x1, local copies, waits for them, and re-layouts: 6.14 us -> 1.26 us
  transfers between devices with their start and end apart: 6 -> 0, of which waited for: 4 -> 0; matrix products, arithmetic and copies ran while one was open for 13% -> 0% of each run, Pallas kernels for 0% -> 0%
where the time goes in v1:
time: 37.5 us; the launch traced here: 37.2 us
  Pallas kernels  35.3 us (94%)
  local copies, waits for them, and re-layouts  1.26 us (3%)
  between operations  0.66 us (2%)
    pallas_call x1, Pallas kernels, fused(): pl.pallas_call(functools.partial(layer_kernel, kv_n, tp_n), out_shape=jax...  35.3 us
    unnamed x1, local copies, waits for them, and re-layouts  1.26 us

profile of v1, /device:TPU:0, one launch (start us, length us, event | category | flops | bytes accessed | tf_op | source)
XLA Modules:
  0.0 37.2 jit_solution(3177341952055892443)
XLA Ops:
  0.7 35.3 %shard_map.253 = bf16[4,256]{1,0:T(4,128)(2,1)} custom-call(s32[1]{0:T(128)S(6)} %copy.29.lengths, bf16[4,256]{1,0:T(4,128)(2,1)} %bitcast.52, f32[1,2048]{1,0:T(1,128)} %bitcast.47, f32[1,64]{1,0:T(1,128)} %bitcast.53, f32[1,64]{1,0:T(1,128)} %bitcast.54, f32[1,64]{1,0:T(1,128)} %bitcast.55, f32[4,32,64]{2,1,0:T(8,128)} %bitcast.43, f32[4,1024]{1,0:T(4,128)} %taps_input.1, ...), custom_call_target="tpu_custom_call" | custom-call | tf_op jit(solution)/shard_map/pallas_call | solution.py:590
  36.0 1.3 %copy.30 = bf16[256,4]{0,1:T(4,128)(2,1)} copy(bf16[256,4]{0,1:T(4,128)(2,1)} %bitcast.51) | data formatting | bytes 4096

commit v2 on v1

--- a/solution.py
+++ b/solution.py
@@ -200,6 +200,34 @@
 def layer_kernel(
     kv_n,
     tp_n,
+    lengths_hbm,
+    hidden_hbm,
+    mixer_gain_hbm,
+    step_bias_hbm,
+    decay_log_hbm,
+    skip_gain_hbm,
+    taps_inner_hbm,
+    taps_input_hbm,
+    taps_output_hbm,
+    recent_inner_hbm,
+    recent_input_hbm,
+    recent_output_hbm,
+    block_decay_hbm,
+    norm_gain_hbm,
+    channel_gain_hbm,
+    gate_hbm,
+    inner_hbm,
+    input_hbm,
+    output_hbm,
+    step_hbm,
+    block_input_hbm,
+    states_hbm,
+    block_inner_hbm,
+    mixer_out_hbm,
+    expand_gate_hbm,
+    expand_value_hbm,
+    reduce_hbm,
+    out,
     lengths,
     hidden,
     mixer_gain,
@@ -215,19 +243,6 @@
     block_decay,
     norm_gain,
     channel_gain,
-    gate_hbm,
-    inner_hbm,
-    input_hbm,
-    output_hbm,
-    step_hbm,
-    block_input_hbm,
-    states_hbm,
-    block_inner_hbm,
-    mixer_out_hbm,
-    expand_gate_hbm,
-    expand_value_hbm,
-    reduce_hbm,
-    out,
     gate_w,
     inner_w,
     input_w,
@@ -271,6 +286,23 @@
     own_ch = channels // kv_n
     own_in = input_w.shape[1]
 
+    small = (
+        (hidden_hbm, hidden),
+        (lengths_hbm, lengths),
+        (taps_inner_hbm, taps_inner),
+        (recent_inner_hbm, recent_inner),
+        (norm_gain_hbm, norm_gain),
+        (block_decay_hbm, block_decay),
+        (taps_input_hbm, taps_input),
+        (recent_input_hbm, recent_input),
+        (taps_output_hbm, taps_output),
+        (recent_output_hbm, recent_output),
+        (step_bias_hbm, step_bias),
+        (decay_log_hbm, decay_log),
+        (skip_gain_hbm, skip_gain),
+        (mixer_gain_hbm, mixer_gain),
+        (channel_gain_hbm, channel_gain),
+    )
     pairs = (
         (output_hbm, output_w),
         (input_hbm, input_w),
@@ -286,7 +318,7 @@
         (reduce_hbm, reduce_w),
     )
     loads = {}
-    for i, (src, dst) in enumerate(pairs):
+    for i, (src, dst) in enumerate(small + pairs):
         copy = pltpu.make_async_copy(src, dst, load_sem.at[i])
         copy.start()
         loads[id(dst)] = copy
@@ -340,9 +372,12 @@
         pending.extend(copies)
         return copies
 
+    loads[id(hidden)].wait()
     gather = to_all(0, lambda other: hidden, hid_all)
     hid_all[me] = hidden[...]
 
+    for _, ref in small[1:]:
+        loads[id(ref)].wait()
     column = lax.broadcasted_iota(jnp.int32, (heads, channels), 1)
     row = lax.broadcasted_iota(jnp.int32, (heads, channels), 0)
     head_mask[...] = jnp.where(
@@ -513,7 +548,7 @@
     added = last_recv[0]
     for i in range(1, n):
         added = added + last_recv[i]
-    out[...] = (mid + added).astype(out.dtype)
+    out[...] = mid + added
     for copy in pending:
         copy.wait_send()
 
@@ -589,12 +624,11 @@
     pre = 2 * own_in + 2 * own_ch
     result = pl.pallas_call(
         functools.partial(layer_kernel, kv_n, tp_n),
-        out_shape=jax.ShapeDtypeStruct((seqs, rows), hidden.dtype),
-        in_specs=[pl.BlockSpec(memory_space=pltpu.SMEM)]
-        + [pl.BlockSpec(memory_space=pltpu.VMEM)] * len(small)
-        + [pl.BlockSpec(memory_space=pl.ANY)] * len(large),
+        out_shape=jax.ShapeDtypeStruct((seqs, rows), F32),
+        in_specs=[pl.BlockSpec(memory_space=pl.ANY)] * (1 + len(small) + len(large)),
         out_specs=pl.BlockSpec(memory_space=pltpu.VMEM),
-        scratch_shapes=[pltpu.VMEM(a.shape, a.dtype) for a in large]
+        scratch_shapes=[pltpu.SMEM(lengths.shape, lengths.dtype)]
+        + [pltpu.VMEM(a.shape, a.dtype) for a in small + large]
         + [
             pltpu.VMEM((heads, channels), F32),
             pltpu.VMEM((n, seqs, rows), hidden.dtype),
@@ -608,7 +642,7 @@
             pltpu.VMEM((n, seqs, rows), F32),
             pltpu.VMEM((n, seqs, rows), F32),
             pltpu.VMEM((n, seqs, rows), F32),
-            pltpu.SemaphoreType.DMA((len(large),)),
+            pltpu.SemaphoreType.DMA((1 + len(small) + len(large),)),
             pltpu.SemaphoreType.DMA((6 * n,)),
             pltpu.SemaphoreType.DMA((6 * n,)),
         ],
@@ -616,7 +650,7 @@
             collective_id=0, has_side_effects=True, vmem_limit_bytes=56 * 1024 * 1024
         ),
     )(lengths, *small, *large)
-    return result.T
+    return result.T.astype(hidden.dtype)
 
 
 def wide_enough(kv_n, tp_n, args):

time: 37.5 us -> 36.7 us (0.979)
  other arithmetic: 0 us -> 1.26 us
  local copies, waits for them, and re-layouts: 1.26 us -> 0 us
  Pallas kernels: 35.3 us -> 34.6 us
    unnamed x1 -> x0, local copies, waits for them, and re-layouts: 1.26 us -> none
    convert_element_type x0 -> x1, other arithmetic: none -> 1.26 us  [fused(): return result.T.astype(hidden.dtype)]
    pallas_call x1, Pallas kernels: 35.3 us -> 34.6 us  [fused(): pl.pallas_call(functools.partial(layer_kernel, kv_n, tp_n), out_shape=jax...]
where the time goes in v2:
time: 36.7 us; the launch traced here: 36.5 us
  Pallas kernels  34.6 us (94%)
  other arithmetic  1.26 us (3%)
  between operations  0.66 us (2%)
    pallas_call x1, Pallas kernels, fused(): pl.pallas_call(functools.partial(layer_kernel, kv_n, tp_n), out_shape=jax...  34.6 us
    convert_element_type x1, other arithmetic, fused(): return result.T.astype(hidden.dtype)  1.26 us

profile of v2, /device:TPU:0, one launch (start us, length us, event | category | flops | bytes accessed | tf_op | source)
XLA Modules:
  0.0 36.5 jit_solution(3860132586344734691)
XLA Ops:
  0.7 34.6 %shard_map.253 = f32[4,256]{1,0:T(4,128)} custom-call(s32[1]{0:T(128)S(6)} %copy.28.lengths_hbm, bf16[4,256]{1,0:T(4,128)(2,1)} %bitcast.52, f32[1,2048]{1,0:T(1,128)} %bitcast.48, f32[1,64]{1,0:T(1,128)} %bitcast.53, f32[1,64]{1,0:T(1,128)} %bitcast.54, f32[1,64]{1,0:T(1,128)} %bitcast.55, f32[4,32,64]{2,1,0:T(8,128)} %bitcast.44, ...), custom_call_target="tpu_custom_call" | custom-call | tf_op jit(solution)/shard_map/pallas_call | solution.py:625
  35.2 1.3 %convert_bitcast_fusion = bf16[256,4]{0,1:T(4,128)(2,1)} fusion(f32[4,256]{1,0:T(4,128)} %shard_map.253), kind=kLoop, calls=%fused_computation | loop fusion | flops 1024 | bytes 6144 | tf_op jit(solution)/shard_map/convert_element_type | solution.py:653

commit v3 on v2

--- a/solution.py
+++ b/solution.py
@@ -338,21 +338,38 @@
 
     pending = []
 
+    def far_first(k, own, count):
+        down = count - 1 - k
+        down = down - jnp.where(down <= own, 1, 0)
+        up = k + jnp.where(k >= own, 1, 0)
+        return jnp.where(2 * own < count, down, up)
+
     def to_all(phase, src_of, dst):
         copies = []
-        for k in range(1, n):
-            other, where = peer(k)
+        for k in range(n - 1):
+            other = far_first(k, me, n)
             copy = pltpu.make_async_remote_copy(
                 src_ref=src_of(other),
                 dst_ref=dst.at[me],
                 send_sem=send_sem.at[phase * n + k],
-                recv_sem=recv_sem.at[phase * n + k],
-                device_id=where,
+                recv_sem=recv_sem.at[phase * n + me],
+                device_id={"kv": other // tp_n, "tp": lax.rem(other, tp_n)},
                 device_id_type=MESH,
             )
             copy.start()
-            copies.append(copy)
-        pending.extend(copies)
+            pending.append(copy)
+        for k in range(1, n):
+            other, where = peer(k)
+            copies.append(
+                pltpu.make_async_remote_copy(
+                    src_ref=src_of(other),
+                    dst_ref=dst.at[other],
+                    send_sem=send_sem.at[phase * n + k - 1],
+                    recv_sem=recv_sem.at[phase * n + other],
+                    device_id=where,
+                    device_id_type=MESH,
+                )
+            )
         return copies
 
     def to_line(phase, src, dst):

time: 36.7 us -> 36.6 us (level)
  no operation moved by 1% of the time
where the time goes in v3:
time: 36.6 us; the launch traced here: 36.4 us
  Pallas kernels  34.5 us (94%)
  other arithmetic  1.26 us (3%)
  between operations  0.66 us (2%)
    pallas_call x1, Pallas kernels, fused(): pl.pallas_call(functools.partial(layer_kernel, kv_n, tp_n), out_shape=jax...  34.5 us
    convert_element_type x1, other arithmetic, fused(): return result.T.astype(hidden.dtype)  1.26 us

profile of v3, /device:TPU:0, one launch (start us, length us, event | category | flops | bytes accessed | tf_op | source)
XLA Modules:
  0.0 36.4 jit_solution(2289074446826634397)
XLA Ops:
  0.7 34.5 %shard_map.253 = f32[4,256]{1,0:T(4,128)} custom-call(s32[1]{0:T(128)S(6)} %copy.28.lengths_hbm, bf16[4,256]{1,0:T(4,128)(2,1)} %bitcast.52, f32[1,2048]{1,0:T(1,128)} %bitcast.48, f32[1,64]{1,0:T(1,128)} %bitcast.53, f32[1,64]{1,0:T(1,128)} %bitcast.54, f32[1,64]{1,0:T(1,128)} %bitcast.55, f32[4,32,64]{2,1,0:T(8,128)} %bitcast.44, ...), custom_call_target="tpu_custom_call" | custom-call | tf_op jit(solution)/shard_map/pallas_call | solution.py:642
  35.1 1.3 %convert_bitcast_fusion = bf16[256,4]{0,1:T(4,128)(2,1)} fusion(f32[4,256]{1,0:T(4,128)} %shard_map.253), kind=kLoop, calls=%fused_computation | loop fusion | flops 1024 | bytes 6144 | tf_op jit(solution)/shard_map/convert_element_type | solution.py:670
